TPU v7x, 32 devices: a whole 2x2x4 slice. The times are simulated.
32 devices in a mesh: fs: 4 (over z), rep: 4 (over y, x), tp: 2 (over core).
Axes of the slice: x: 2, y: 2, z: 4, core: 2. Of those that a mesh axis runs over, the one named last changes fastest.
Arguments:
- saved_latent: bfloat16 [12288, 2048], P(('fs', 'rep')), may hold values from -6 to 6
- query_cotangent: bfloat16 [12288, 3072], P(('fs', 'rep'), 'tp'), may hold values from -6 to 6
- mix_cotangent: bfloat16 [12288, 4096], P(('fs', 'rep')), may hold values from -6 to 6
- head_outputs: bfloat16 [12288, 2048], P(('fs', 'rep'), 'tp'), may hold values from -6 to 6
- query_weight: float32 [2048, 3072], P('fs', 'tp'), may hold values from -0.125 to 0.125
- out_weight: float32 [4096, 2048], P('fs', 'tp'), may hold values from -0.125 to 0.125
- query_basis: bfloat16 [2048, 256], replicated, may hold values from -0.125 to 0.125
- out_basis: bfloat16 [4096, 256], replicated, may hold values from -0.09375 to 0.09375
- query_mean: float32 [256, 3072], P('fs', 'tp'), may hold values from -3 to 3
- query_var: float32 [256, 3072], P('fs', 'tp'), may hold values from 0.1 to 1
- out_mean: float32 [256, 2048], P('fs', 'tp'), may hold values from -3 to 3
- out_var: float32 [256, 2048], P('fs', 'tp'), may hold values from 0.1 to 1
Outputs:
- query_step: float32 [2048, 3072], P('fs', 'tp')
- out_step: float32 [4096, 2048], P('fs', 'tp')
- query_copy: bfloat16 [2048, 3072], P('fs', 'tp')
- out_copy: bfloat16 [4096, 2048], P('fs', 'tp')
All inputs are finite; a program needn't handle non-finite values.
Results may differ from a plain program's by a relative error of at most 0.001.
Values sent between devices are 32-bit elements; how exact they have to be, the bound alone decides.
A program may use at most 128 MiB of HBM per device.

v0:
```python
import jax
import jax.numpy as jnp
from jax import lax
from jax.sharding import PartitionSpec as P


def token_sum(left, right):
    return lax.dot_general(
        left, right, (((0,), (0,)), ((), ())), preferred_element_type=jnp.float32
    )


def project(basis, grad):
    return lax.dot_general(
        basis.astype(jnp.float32), grad, (((0,), (0,)), ((), ())), precision=lax.Precision.HIGHEST
    )


def moment_direction(proj, scale, mean, var):
    scaled = scale * proj
    new_mean = 0.8 * mean + 0.2 * scaled
    new_var = 0.9 * var + 0.1 * scaled * scaled
    return new_mean / jnp.sqrt(new_var)


def on_device(
    saved_latent,
    query_cotangent,
    mix_cotangent,
    head_outputs,
    query_weight,
    out_weight,
    query_basis,
    out_basis,
    query_mean,
    query_var,
    out_mean,
    out_var,
):
    query_rows = query_weight.shape[0]
    out_rows = out_weight.shape[0]
    position = lax.axis_index("fs")
    query_local = lax.dynamic_slice_in_dim(query_basis, position * query_rows, query_rows, 0)
    out_local = lax.dynamic_slice_in_dim(out_basis, position * out_rows, out_rows, 0)
    query_early = project(query_basis, token_sum(saved_latent, query_cotangent))
    out_early = project(out_basis, token_sum(mix_cotangent, head_outputs))
    query_shard, out_shard = (
        lax.psum_scatter(query_early, "fs", scatter_dimension=0, tiled=True),
        lax.psum_scatter(out_early, "fs", scatter_dimension=0, tiled=True),
    )
    query_proj, out_proj = lax.psum((query_shard, out_shard), "rep")
    query_squares, out_squares = lax.psum(
        (jnp.sum(query_proj * query_proj), jnp.sum(out_proj * out_proj)), ("fs", "tp")
    )
    spread = lax.axis_size("fs") * lax.axis_size("tp")
    query_count = float(query_proj.shape[0] * query_proj.shape[1] * spread)
    out_count = float(out_proj.shape[0] * out_proj.shape[1] * spread)
    query_scale = 1.0 / jnp.maximum(jnp.sqrt(query_squares / query_count), 1.0)
    out_scale = 1.0 / jnp.maximum(jnp.sqrt(out_squares / out_count), 1.0)
    query_dir = moment_direction(query_proj, query_scale, query_mean, query_var)
    out_dir = moment_direction(out_proj, out_scale, out_mean, out_var)
    query_left = query_local.astype(jnp.float32)
    out_left = out_local.astype(jnp.float32)
    query_step = jnp.dot(
        query_left,
        lax.all_gather(query_dir, "fs", axis=0, tiled=True),
        precision=lax.Precision.HIGHEST,
    )
    out_step = jnp.dot(
        out_left, lax.all_gather(out_dir, "fs", axis=0, tiled=True), precision=lax.Precision.HIGHEST
    )
    query_copy = (query_weight - 0.05 * query_step).astype(jnp.bfloat16)
    out_copy = (out_weight - 0.05 * out_step).astype(jnp.bfloat16)
    return (query_step, out_step, query_copy, out_copy)


def solution(mesh):
    placed = (
        P(("fs", "rep"), None),
        P(("fs", "rep"), "tp"),
        P(("fs", "rep"), None),
        P(("fs", "rep"), "tp"),
        P("fs", "tp"),
        P("fs", "tp"),
        P(),
        P(),
        P("fs", "tp"),
        P("fs", "tp"),
        P("fs", "tp"),
        P("fs", "tp"),
    )
    return jax.shard_map(
        on_device,
        mesh=mesh,
        in_specs=placed,
        out_specs=(P("fs", "tp"), P("fs", "tp"), P("fs", "tp"), P("fs", "tp")),
        check_vma=False,
    )
```

profile of v0, /device:TPU:0, one launch (start us, length us, event | category | flops | bytes accessed | tf_op | source)
XLA Modules:
  0.0 259.1 jit_solution(1730076010502316369)
XLA Ops:
  7.2 0.0 reduce-scatter.9.cloned.1.call-start
  7.2 9.9 %fusion.13 = f32[4096,1024]{1,0:T(8,128)S(1)} fusion(bf16[768,4096]{1,0:T(8,128)(2,1)} %param.14, bf16[768,1024]{1,0:T(8,128)(2,1)} %param.15), kind=kOutput, calls=%fused_computation.21 | convolution fusion | flops 6442450944 | bytes 24641536 | tf_op jit(solution)/shard_map/dot_general | solution.py:8
  17.1 24.0 %convolution_bitcast_fusion.1 = f32[256,1024]{0,1:T(8,128)} fusion(f32[4096,1024]{1,0:T(8,128)S(1)} %fusion.13, bf16[4096,256]{1,0:T(8,128)(2,1)S(1)} %copy-done.2), kind=kOutput, calls=%fused_computation.3 | convolution fusion | flops 12884901888 | bytes 19922944 | tf_op jit(solution)/shard_map/dot_general | solution.py:14
  41.2 2.5 copy.30
  43.7 0.0 reduce-scatter.9.cloned.1.call-update
  43.7 0.0 reduce-scatter.7.cloned.1.call-start
  43.8 7.0 %fusion.12 = f32[2048,1536]{1,0:T(8,128)S(1)} fusion(bf16[768,2048]{1,0:T(8,128)(2,1)S(1)} %copy-done, bf16[768,1536]{1,0:T(8,128)(2,1)} %param.13), kind=kOutput, calls=%fused_computation.20 | convolution fusion | flops 4831838208 | bytes 18087936 | tf_op jit(solution)/shard_map/dot_general | solution.py:8
  50.8 10.6 %convolution_bitcast_fusion = f32[256,1536]{0,1:T(8,128)S(1)} fusion(f32[2048,1536]{1,0:T(8,128)S(1)} %fusion.12, bf16[2048,256]{1,0:T(8,128)(2,1)S(1)} %copy-done.3), kind=kOutput, calls=%fused_computation.2 | convolution fusion | flops 9663676416 | bytes 15204352 | tf_op jit(solution)/shard_map/dot_general | solution.py:14
  61.5 1.6 copy.28
  63.1 0.0 all-reduce.4.cloned.1.call-start
  63.2 10.7 %reduce-scatter.9.cloned.1.call-done = f32[64,1024]{1,0:T(8,128)} async-done(((f32[256,1024]{1,0:T(8,128)}), f32[64,1024]{1,0:T(8,128)}) %reduce-scatter.9.cloned.1.call-update) | async-done | bytes 262160 | tf_op jit(solution)/shard_map/reduce_scatter | solution.py:49
  73.9 36.9 %reduce-scatter.7.cloned.1.call-done = f32[64,1536]{1,0:T(8,128)} async-done(((f32[256,1536]{1,0:T(8,128)}), f32[64,1536]{1,0:T(8,128)}) %reduce-scatter.7.cloned.1.call-update) | async-done | bytes 393232 | tf_op jit(solution)/shard_map/reduce_scatter | solution.py:48
  110.7 0.0 all-gather.5.cloned.1.call-start
  110.8 48.7 %all-reduce.4.cloned.1.call-done = (f32[64,1536]{1,0:T(8,128)}, f32[64,1024]{1,0:T(8,128)}) async-done(((f32[64,1536]{1,0:T(8,128)}, f32[64,1024]{1,0:T(8,128)}), (f32[64,1536]{1,0:T(8,128)}, f32[64,1024]{1,0:T(8,128)})) %all-reduce.4.cloned.1.call-update) | async-done | bytes 655376 | tf_op jit(solution)/shard_map/psum | solution.py:51
  159.5 1.7 multiply_reduce_fusion
  161.2 1.6 multiply_reduce_fusion.1
  162.8 16.9 %all-reduce = (f32[]{:T(128)}, f32[]{:T(128)}) all-reduce(f32[]{:T(128)} %multiply_reduce_fusion, f32[]{:T(128)} %multiply_reduce_fusion.1), channel_id=1, replica_groups=mesh['fs'=4,'rep'=4,'tp'=2] {'fs','tp'}, use_global_device_ids=true, to_apply=%region_3.0 | all-reduce | flops 2 | bytes 16 | tf_op jit(solution)/shard_map/psum | solution.py:52
  180.5 1.7 fusion.7
  182.2 0.0 all-gather.3.cloned.1.call-start
  183.0 1.9 fusion.4
  184.9 22.7 %all-gather.5.cloned.1.call-done = f32[256,1024]{1,0:T(8,128)} async-done(((f32[64,1024]{1,0:T(8,128)}), f32[256,1024]{1,0:T(8,128)}) %all-gather.5.cloned.1.call-update) | async-done | bytes 1048592 | tf_op jit(solution)/shard_map/all_gather | solution.py:70
  207.6 7.6 %subtract_convert_fusion = (bf16[1024,1024]{1,0:T(8,128)(2,1)}, f32[1024,1024]{1,0:T(8,128)}) fusion(f32[1024,1024]{1,0:T(8,128)} %param.17, f32[256,1024]{1,0:T(8,128)} %all-gather.5.cloned.1.call-done, bf16[4096,256]{1,0:T(8,128)(2,1)} %param.19, s32[]{:T(128)S(6)} %select_n.7), kind=kOutput, calls=%fused_computation | convolution fusion | flops 3224371200 | bytes 12058628 | tf_op jit(solution)/shard_map/dot_general | solution.py:69
  215.2 30.8 %all-gather.3.cloned.1.call-done = f32[256,1536]{1,0:T(8,128)} async-done(((f32[64,1536]{1,0:T(8,128)}), f32[256,1536]{1,0:T(8,128)}) %all-gather.3.cloned.1.call-update) | async-done | bytes 1572880 | tf_op jit(solution)/shard_map/all_gather | solution.py:66
  246.0 6.3 %subtract_convert_fusion.1 = (bf16[512,1536]{1,0:T(8,128)(2,1)}, f32[512,1536]{1,0:T(8,128)}) fusion(f32[512,1536]{1,0:T(8,128)} %param.16, f32[256,1536]{1,0:T(8,128)} %all-gather.3.cloned.1.call-done, bf16[2048,256]{1,0:T(8,128)(2,1)} %param.18, s32[]{:T(128)S(6)} %select_n.6), kind=kOutput, calls=%fused_computation.1 | convolution fusion | flops 2418278400 | bytes 9699332 | tf_op jit(solution)/shard_map/dot_general | solution.py:64
  (20 shorter events, 0.1 us)
Async XLA Ops:
  7.2 36.6 %copy-start = (bf16[768,2048]{1,0:T(8,128)(2,1)S(1)}, bf16[768,2048]{1,0:T(8,128)(2,1)}, u32[]{:S(2)}) copy-start(bf16[768,2048]{1,0:T(8,128)(2,1)} %param.12) | copy-start | bytes 9437188
  7.2 66.7 %reduce-scatter.9.cloned.1.call-start = ((), (), s32[]{:S(2)}) async-start(), calls=%async_computation.5 | async-start | bytes 1310720 | tf_op jit(solution)/shard_map/reduce_scatter | solution.py:49
  7.2 9.9 %copy-start.2 = (bf16[4096,256]{1,0:T(8,128)(2,1)S(1)}, bf16[4096,256]{1,0:T(8,128)(2,1)}, u32[]{:S(2)}) copy-start(bf16[4096,256]{1,0:T(8,128)(2,1)} %param.19) | copy-start | bytes 6291460
  43.7 67.0 %reduce-scatter.7.cloned.1.call-start = ((), (), s32[]{:S(2)}) async-start(), calls=%async_computation.4 | async-start | bytes 1966080 | tf_op jit(solution)/shard_map/reduce_scatter | solution.py:48
  43.8 7.1 %copy-start.3 = (bf16[2048,256]{1,0:T(8,128)(2,1)S(1)}, bf16[2048,256]{1,0:T(8,128)(2,1)}, u32[]{:S(2)}) copy-start(bf16[2048,256]{1,0:T(8,128)(2,1)} %param.18) | copy-start | bytes 3145732
  61.4 119.0 %copy-start.6 = (f32[64,1024]{1,0:T(8,128)S(1)}, f32[64,1024]{1,0:T(8,128)}, u32[]{:S(2)}) copy-start(f32[64,1024]{1,0:T(8,128)} %param.23) | copy-start | bytes 786436
  61.4 119.0 %copy-start.7 = (f32[64,1024]{1,0:T(8,128)S(1)}, f32[64,1024]{1,0:T(8,128)}, u32[]{:S(2)}) copy-start(f32[64,1024]{1,0:T(8,128)} %param.22) | copy-start | bytes 786436
  61.4 121.6 %copy-start.4 = (f32[64,1536]{1,0:T(8,128)S(1)}, f32[64,1536]{1,0:T(8,128)}, u32[]{:S(2)}) copy-start(f32[64,1536]{1,0:T(8,128)} %param.21) | copy-start | bytes 1179652
  61.5 121.6 %copy-start.5 = (f32[64,1536]{1,0:T(8,128)S(1)}, f32[64,1536]{1,0:T(8,128)}, u32[]{:S(2)}) copy-start(f32[64,1536]{1,0:T(8,128)} %param.20) | copy-start | bytes 1179652
  63.1 96.4 %all-reduce.4.cloned.1.call-start = ((), (), s32[]{:S(2)}) async-start(), calls=%async_computation.6 | async-start | bytes 1310720 | tf_op jit(solution)/shard_map/psum | solution.py:51
  110.7 96.9 %all-gather.5.cloned.1.call-start = ((), (), s32[]{:S(2)}) async-start(), calls=%async_computation.3 | async-start | bytes 1310720 | tf_op jit(solution)/shard_map/all_gather | solution.py:70
  182.2 63.8 %all-gather.3.cloned.1.call-start = ((), (), s32[]{:S(2)}) async-start(), calls=%async_computation.2 | async-start | bytes 1966080 | tf_op jit(solution)/shard_map/all_gather | solution.py:66
  207.6 44.7 %copy-start.1 = (bf16[768,2048]{1,0:T(8,128)(2,1)S(1)}, bf16[768,2048]{1,0:T(8,128)(2,1)}, u32[]{:S(2)}) copy-start(bf16[768,2048]{1,0:T(8,128)(2,1)} %param.12) | copy-start | bytes 9437188
Sparse Core Ops, SparseCore 0:
  43.8 29.9 reduce-scatter.8
  76.7 33.9 reduce-scatter.6
  113.8 45.6 all-reduce.3
  182.4 25.2 all-gather.4
  209.6 36.3 all-gather.2
where the time goes:
time: 262 us; the launch traced here: 259 us
  waiting for transfers between devices  150 us (57%)
  matrix products  65.4 us (25%)
  blocking collectives  16.9 us (6%)
  between operations  15.6 us (6%)
  other arithmetic  6.95 us (3%)
  local copies, waits for them, and re-layouts  4.2 us (2%)
    psum x1, waiting for transfers between devices, on_device(): query_proj, out_proj = lax.psum((query_shard, out_shard), 'rep')  48.7 us
    reduce_scatter x1, waiting for transfers between devices, on_device(): lax.psum_scatter(query_early, 'fs', scatter_dimension=0, tiled=True)  36.9 us
    dot_general x2, matrix products, project(): lax.dot_general(basis.astype(jnp.float32), grad, (((0,), (0,)), ((), ()))...  34.6 us
    all_gather x1, waiting for transfers between devices, on_device(): lax.all_gather(query_dir, 'fs', axis=0, tiled=True)  30.8 us
    all_gather x1, waiting for transfers between devices, on_device(): lax.all_gather(out_dir, 'fs', axis=0, tiled=True)  22.7 us
    dot_general x2, matrix products, token_sum(): lax.dot_general(left, right, (((0,), (0,)), ((), ())), preferred_element_...  16.9 us
    psum x1, blocking collectives, on_device(): lax.psum((jnp.sum(query_proj * query_proj), jnp.sum(out_proj * out_proj))...  16.9 us
    reduce_scatter x1, waiting for transfers between devices, on_device(): lax.psum_scatter(out_early, 'fs', scatter_dimension=0, tiled=True)  10.7 us
  transfers between devices with their start and end apart: 5, of which 5 were waited for; matrix products, arithmetic and copies ran while one was open for 11% of the time, Pallas kernels for 0%

commit v1 on v0

--- a/solution.py
+++ b/solution.py
@@ -2,6 +2,7 @@
 import jax.numpy as jnp
 from jax import lax
 from jax.sharding import PartitionSpec as P
+from jax.lax import all_to_all, axis_size
 
 
 def token_sum(left, right):
@@ -63,7 +64,15 @@
     out_left = out_local.astype(jnp.float32)
     query_step = jnp.dot(
         query_left,
-        lax.all_gather(query_dir, "fs", axis=0, tiled=True),
+        jnp.concatenate(
+            all_to_all(
+                jnp.stack([query_dir] * axis_size("fs"), axis=0),
+                axis_name="fs",
+                concat_axis=0,
+                split_axis=0,
+            ),
+            axis=0,
+        ),
         precision=lax.Precision.HIGHEST,
     )
     out_step = jnp.dot(

time: 262 us -> 260 us (level)
  waiting for transfers between devices: 150 us -> 143 us
  starting transfers between devices: 0.2 us -> 4.51 us
    all_gather x1 -> x0, waiting for transfers between devices: 30.8 us -> none  [on_device(): lax.all_gather(query_dir, 'fs', axis=0, tiled=True)]
    all_gather x1, waiting for transfers between devices: 22.7 us -> 46.5 us  [on_device(): lax.all_gather(out_dir, 'fs', axis=0, tiled=True)]
    all_to_all x0 -> x1, starting transfers between devices: none -> 4.35 us  [on_device(): all_to_all(jnp.stack([query_dir] * axis_size('fs'), axis=0), axis_name='f...]
  transfers between devices with their start and end apart: 5 -> 5, of which waited for: 5 -> 4; matrix products, arithmetic and copies ran while one was open for 11% -> 11% of each run, Pallas kernels for 0% -> 0%
where the time goes in v1:
time: 260 us; the launch traced here: 256 us
  waiting for transfers between devices  143 us (55%)
  matrix products  65.4 us (25%)
  blocking collectives  16.9 us (6%)
  between operations  15.6 us (6%)
  local copies, waits for them, and re-layouts  5.53 us (2%)
  other arithmetic  5.32 us (2%)
  starting transfers between devices  4.51 us (2%)
    psum x1, waiting for transfers between devices, on_device(): query_proj, out_proj = lax.psum((query_shard, out_shard), 'rep')  48.7 us
    all_gather x1, waiting for transfers between devices, on_device(): lax.all_gather(out_dir, 'fs', axis=0, tiled=True)  46.5 us
    reduce_scatter x1, waiting for transfers between devices, on_device(): lax.psum_scatter(query_early, 'fs', scatter_dimension=0, tiled=True)  36.9 us
    dot_general x2, matrix products, project(): lax.dot_general(basis.astype(jnp.float32), grad, (((0,), (0,)), ((), ()))...  34.6 us
    dot_general x2, matrix products, token_sum(): lax.dot_general(left, right, (((0,), (0,)), ((), ())), preferred_element_...  16.9 us
    psum x1, blocking collectives, on_device(): lax.psum((jnp.sum(query_proj * query_proj), jnp.sum(out_proj * out_proj))...  16.9 us
    reduce_scatter x1, waiting for transfers between devices, on_device(): lax.psum_scatter(out_early, 'fs', scatter_dimension=0, tiled=True)  10.7 us
    dot_general x1, matrix products, on_device(): jnp.dot(out_left, lax.all_gather(out_dir, 'fs', axis=0, tiled=True), prec...  7.46 us
  transfers between devices with their start and end apart: 5, of which 4 were waited for; matrix products, arithmetic and copies ran while one was open for 11% of the time, Pallas kernels for 0%

profile of v1, /device:TPU:0, one launch (start us, length us, event | category | flops | bytes accessed | tf_op | source)
XLA Modules:
  0.0 256.2 jit_solution(6766477965576251430)
XLA Ops:
  7.2 0.0 reduce-scatter.9.cloned.1.call-start
  7.2 9.9 %fusion.13 = f32[4096,1024]{1,0:T(8,128)S(1)} fusion(bf16[768,4096]{1,0:T(8,128)(2,1)} %param.14, bf16[768,1024]{1,0:T(8,128)(2,1)} %param.15), kind=kOutput, calls=%fused_computation.21 | convolution fusion | flops 6442450944 | bytes 24641536 | tf_op jit(solution)/shard_map/dot_general | solution.py:9
  17.1 24.0 %convolution_bitcast_fusion.1 = f32[256,1024]{0,1:T(8,128)} fusion(f32[4096,1024]{1,0:T(8,128)S(1)} %fusion.13, bf16[4096,256]{1,0:T(8,128)(2,1)S(1)} %copy-done.2), kind=kOutput, calls=%fused_computation.3 | convolution fusion | flops 12884901888 | bytes 19922944 | tf_op jit(solution)/shard_map/dot_general | solution.py:15
  41.2 2.5 copy.31
  43.7 0.0 reduce-scatter.9.cloned.1.call-update
  43.7 0.0 reduce-scatter.7.cloned.1.call-start
  43.8 7.0 %fusion.12 = f32[2048,1536]{1,0:T(8,128)S(1)} fusion(bf16[768,2048]{1,0:T(8,128)(2,1)S(1)} %copy-done, bf16[768,1536]{1,0:T(8,128)(2,1)} %param.13), kind=kOutput, calls=%fused_computation.20 | convolution fusion | flops 4831838208 | bytes 18087936 | tf_op jit(solution)/shard_map/dot_general | solution.py:9
  50.8 10.6 %convolution_bitcast_fusion = f32[256,1536]{0,1:T(8,128)S(1)} fusion(f32[2048,1536]{1,0:T(8,128)S(1)} %fusion.12, bf16[2048,256]{1,0:T(8,128)(2,1)S(1)} %copy-done.3), kind=kOutput, calls=%fused_computation.2 | convolution fusion | flops 9663676416 | bytes 15204352 | tf_op jit(solution)/shard_map/dot_general | solution.py:15
  61.4 1.6 copy.29
  63.1 0.0 all-reduce.4.cloned.1.call-start
  63.1 10.7 %reduce-scatter.9.cloned.1.call-done = f32[64,1024]{1,0:T(8,128)} async-done(((f32[256,1024]{1,0:T(8,128)}), f32[64,1024]{1,0:T(8,128)}) %reduce-scatter.9.cloned.1.call-update) | async-done | bytes 262160 | tf_op jit(solution)/shard_map/reduce_scatter | solution.py:50
  73.9 36.9 %reduce-scatter.7.cloned.1.call-done = f32[64,1536]{1,0:T(8,128)} async-done(((f32[256,1536]{1,0:T(8,128)}), f32[64,1536]{1,0:T(8,128)}) %reduce-scatter.7.cloned.1.call-update) | async-done | bytes 393232 | tf_op jit(solution)/shard_map/reduce_scatter | solution.py:49
  110.7 48.7 %all-reduce.4.cloned.1.call-done = (f32[64,1536]{1,0:T(8,128)}, f32[64,1024]{1,0:T(8,128)}) async-done(((f32[64,1536]{1,0:T(8,128)}, f32[64,1024]{1,0:T(8,128)}), (f32[64,1536]{1,0:T(8,128)}, f32[64,1024]{1,0:T(8,128)})) %all-reduce.4.cloned.1.call-update) | async-done | bytes 655376 | tf_op jit(solution)/shard_map/psum | solution.py:52
  159.5 1.7 multiply_reduce_fusion
  161.2 1.6 multiply_reduce_fusion.1
  162.8 16.9 %all-reduce = (f32[]{:T(128)}, f32[]{:T(128)}) all-reduce(f32[]{:T(128)} %multiply_reduce_fusion, f32[]{:T(128)} %multiply_reduce_fusion.1), channel_id=1, replica_groups=mesh['fs'=4,'rep'=4,'tp'=2] {'fs','tp'}, use_global_device_ids=true, to_apply=%region_3.0 | all-reduce | flops 2 | bytes 16 | tf_op jit(solution)/shard_map/psum | solution.py:53
  180.5 1.2 fusion.4
  181.7 1.3 stack.2
  183.0 4.3 %all-to-all-start = ((f32[4,64,1536]{2,1,0:T(8,128)}), f32[4,64,1536]{2,1,0:T(8,128)}, u32[]{:S(2)}, u32[]{:S(2)}) async-start(f32[4,64,1536]{2,1,0:T(8,128)} %stack.2), calls=%async_computation | async-start | bytes 3145728 | tf_op jit(solution)/shard_map/all_to_all | solution.py:68
  187.4 0.0 all-gather.2.cloned.1.call-start
  188.2 0.8 fusion.7
  189.0 46.5 %all-gather.2.cloned.1.call-done = f32[256,1024]{1,0:T(8,128)} async-done(((f32[64,1024]{1,0:T(8,128)}), f32[256,1024]{1,0:T(8,128)}) %all-gather.2.cloned.1.call-update) | async-done | bytes 1048592 | tf_op jit(solution)/shard_map/all_gather | solution.py:79
  235.5 7.5 %subtract_convert_fusion = (bf16[1024,1024]{1,0:T(8,128)(2,1)}, f32[1024,1024]{1,0:T(8,128)}) fusion(f32[1024,1024]{1,0:T(8,128)} %param.17, f32[256,1024]{1,0:T(8,128)} %all-gather.2.cloned.1.call-done, bf16[4096,256]{1,0:T(8,128)(2,1)} %param.19, s32[]{:T(128)S(6)} %select_n.7), kind=kOutput, calls=%fused_computation | convolution fusion | flops 3224371200 | bytes 12058628 | tf_op jit(solution)/shard_map/dot_general | solution.py:78
  243.0 6.4 %subtract_convert_fusion.1 = (bf16[512,1536]{1,0:T(8,128)(2,1)}, f32[512,1536]{1,0:T(8,128)}) fusion(f32[512,1536]{1,0:T(8,128)} %param.16, f32[256,1536]{1,0:T(8,128)} %bitcast.1, bf16[2048,256]{1,0:T(8,128)(2,1)} %param.18, s32[]{:T(128)S(6)} %select_n.6), kind=kOutput, calls=%fused_computation.1 | convolution fusion | flops 2418278400 | bytes 9699332 | tf_op jit(solution)/shard_map/dot_general | solution.py:65
  (22 shorter events, 0.1 us)
Async XLA Ops:
  7.2 36.6 %copy-start = (bf16[768,2048]{1,0:T(8,128)(2,1)S(1)}, bf16[768,2048]{1,0:T(8,128)(2,1)}, u32[]{:S(2)}) copy-start(bf16[768,2048]{1,0:T(8,128)(2,1)} %param.12) | copy-start | bytes 9437188
  7.2 66.7 %reduce-scatter.9.cloned.1.call-start = ((), (), s32[]{:S(2)}) async-start(), calls=%async_computation.5 | async-start | bytes 1310720 | tf_op jit(solution)/shard_map/reduce_scatter | solution.py:50
  7.2 9.9 %copy-start.2 = (bf16[4096,256]{1,0:T(8,128)(2,1)S(1)}, bf16[4096,256]{1,0:T(8,128)(2,1)}, u32[]{:S(2)}) copy-start(bf16[4096,256]{1,0:T(8,128)(2,1)} %param.19) | copy-start | bytes 6291460
  43.7 67.0 %reduce-scatter.7.cloned.1.call-start = ((), (), s32[]{:S(2)}) async-start(), calls=%async_computation.4 | async-start | bytes 1966080 | tf_op jit(solution)/shard_map/reduce_scatter | solution.py:49
  43.8 7.1 %copy-start.3 = (bf16[2048,256]{1,0:T(8,128)(2,1)S(1)}, bf16[2048,256]{1,0:T(8,128)(2,1)}, u32[]{:S(2)}) copy-start(bf16[2048,256]{1,0:T(8,128)(2,1)} %param.18) | copy-start | bytes 3145732
  61.4 119.0 %copy-start.5 = (f32[64,1536]{1,0:T(8,128)S(1)}, f32[64,1536]{1,0:T(8,128)}, u32[]{:S(2)}) copy-start(f32[64,1536]{1,0:T(8,128)} %param.21) | copy-start | bytes 1179652
  61.4 119.0 %copy-start.6 = (f32[64,1536]{1,0:T(8,128)S(1)}, f32[64,1536]{1,0:T(8,128)}, u32[]{:S(2)}) copy-start(f32[64,1536]{1,0:T(8,128)} %param.20) | copy-start | bytes 1179652
  63.1 96.4 %all-reduce.4.cloned.1.call-start = ((), (), s32[]{:S(2)}) async-start(), calls=%async_computation.6 | async-start | bytes 1310720 | tf_op jit(solution)/shard_map/psum | solution.py:52
  180.5 7.7 %copy-start.4 = (f32[64,1024]{1,0:T(8,128)S(1)}, f32[64,1024]{1,0:T(8,128)}, u32[]{:S(2)}) copy-start(f32[64,1024]{1,0:T(8,128)} %get-tuple-element.7) | copy-start | bytes 786436
  180.5 7.7 %copy-start.7 = (f32[64,1024]{1,0:T(8,128)S(1)}, f32[64,1024]{1,0:T(8,128)}, u32[]{:S(2)}) copy-start(f32[64,1024]{1,0:T(8,128)} %param.23) | copy-start | bytes 786436
  180.5 7.7 %copy-start.8 = (f32[64,1024]{1,0:T(8,128)S(1)}, f32[64,1024]{1,0:T(8,128)}, u32[]{:S(2)}) copy-start(f32[64,1024]{1,0:T(8,128)} %param.22) | copy-start | bytes 786436
  183.0 60.0 %all-to-all-start = ((f32[4,64,1536]{2,1,0:T(8,128)}), f32[4,64,1536]{2,1,0:T(8,128)}, u32[]{:S(2)}, u32[]{:S(2)}) async-start(f32[4,64,1536]{2,1,0:T(8,128)} %stack.2), calls=%async_computation | async-start | bytes 3145728 | tf_op jit(solution)/shard_map/all_to_all | solution.py:68
  187.4 48.1 %all-gather.2.cloned.1.call-start = ((), (), s32[]{:S(2)}) async-start(), calls=%async_computation.3 | async-start | bytes 1310720 | tf_op jit(solution)/shard_map/all_gather | solution.py:79
  243.0 6.4 %copy-start.1 = (bf16[768,2048]{1,0:T(8,128)(2,1)S(1)}, bf16[768,2048]{1,0:T(8,128)(2,1)}, u32[]{:S(2)}) copy-start(bf16[768,2048]{1,0:T(8,128)(2,1)} %param.12) | copy-start | bytes 9437188
Sparse Core Ops, SparseCore 0:
  43.8 29.9 reduce-scatter.8
  76.7 33.9 reduce-scatter.6
  113.8 45.6 all-reduce.3
  190.0 45.4 all-gather.1
